TPU v7x, 32 devices: a whole 2x2x4 slice. The times are simulated.
32 devices in a mesh: fs: 16 (over z, y, x), tp: 2 (over core).
Axes of the slice: x: 2, y: 2, z: 4, core: 2. Of those that a mesh axis runs over, the one named last changes fastest.
Arguments:
- tokens: bfloat16 [12288, 2048], P('fs'), may hold values from -6 to 6
- norm_gain: float32 [2048], replicated, may hold values from 0.1 to 1.9
- up_weight: float32 [2048, 8192], P('fs', 'tp'), may hold values from -0.125 to 0.125
- up_scale: float32 [8192], P('tp'), may hold values from 0.5 to 2
- down_weight: float32 [8192, 2048], P('tp', 'fs'), may hold values from -0.09375 to 0.09375
- down_scale: float32 [1, 2048], replicated, may hold values from 0.5 to 2
Outputs:
- mixed: bfloat16 [12288, 2048], P('fs', 'tp')
All inputs are finite; a program needn't handle non-finite values.
Results may differ from a plain program's by a relative error of at most 0.014.
Values may be sent and summed in bfloat16 or wider, within the bound.
A program may use at most 128 MiB of HBM per device.

v0:
```python
import jax
import jax.numpy as jnp
from jax import lax
from jax.sharding import PartitionSpec as P


def on_device(tokens, norm_gain, up_weight, up_scale, down_weight, down_scale):
    values = tokens.astype(jnp.float32)
    normed = (
        values * lax.rsqrt(jnp.mean(values * values, axis=-1, keepdims=True) + 1e-06) * norm_gain
    ).astype(jnp.bfloat16)
    up_cast = up_weight.astype(jnp.bfloat16)
    down_cast = down_weight.astype(jnp.bfloat16)
    up_full = lax.all_gather(up_cast, "fs", axis=0, tiled=True)
    pre = jnp.dot(normed, up_full, preferred_element_type=jnp.float32) * up_scale
    hidden = jnp.square(jnp.maximum(pre, 0.0)).astype(jnp.bfloat16)
    down_full = lax.all_gather(down_cast, "fs", axis=1, tiled=True)
    partial_value = jnp.dot(hidden, down_full, preferred_element_type=jnp.float32) * down_scale
    rounded = partial_value.astype(jnp.bfloat16)
    return (
        lax.psum_scatter(rounded, "tp", scatter_dimension=1, tiled=True)
        .astype(jnp.float32)
        .astype(jnp.bfloat16)
    )


def solution(mesh):
    in_specs = (P("fs", None), P(), P("fs", "tp"), P("tp"), P("tp", "fs"), P())
    out_specs = P("fs", "tp")
    return jax.shard_map(
        on_device, mesh=mesh, in_specs=in_specs, out_specs=out_specs, check_vma=False
    )
```

profile of v0, /device:TPU:1, one launch (start us, length us, event | category | flops | bytes accessed | tf_op | source)
XLA Modules:
  0.0 507.9 jit_solution(3920290398394496879)
XLA Ops:
  6.5 0.0 copy-start
  6.5 0.0 copy-start.2
  6.5 0.0 copy-start.1
  6.5 0.0 copy-start.3
  6.5 0.0 all-gather.3.cloned.1.call-start
  6.6 2.8 convert_element_type.22
  9.4 0.0 all-gather.3.cloned.1.call-update
  9.5 0.0 all-gather.5.cloned.1.call-start
  9.5 2.7 convert_element_type.24
  12.2 0.0 all-gather.5.cloned.1.call-update
  12.2 0.0 reduce-scatter.2.cloned.1.call-start
  12.2 0.0 copy-done
  12.3 0.7 fusion
  13.0 189.5 %all-gather.3.cloned.1.call-done = bf16[2048,4096]{1,0:T(8,128)(2,1)} async-done(((bf16[128,4096]{1,0:T(8,128)(2,1)}), bf16[2048,4096]{1,0:T(8,128)(2,1)}) %all-gather.3.cloned.1.call-update) | async-done | bytes 16777232 | tf_op jit(solution)/shard_map/all_gather | solution.py:14
  202.5 250.0 %all-gather.5.cloned.1.call-done = bf16[4096,2048]{1,0:T(8,128)(2,1)} async-done(((bf16[4096,128]{1,0:T(8,128)(2,1)}), bf16[4096,2048]{1,0:T(8,128)(2,1)}) %all-gather.5.cloned.1.call-update) | async-done | bytes 16777232 | tf_op jit(solution)/shard_map/all_gather | solution.py:17
  452.5 0.0 copy-done.2
  452.5 0.0 copy-done.1
  452.5 0.0 copy-done.3
  452.5 38.3 %multiply_convert_fusion.1 = bf16[768,2048]{1,0:T(8,128)(2,1)} fusion(bf16[4096,2048]{1,0:T(8,128)(2,1)} %all-gather.5.cloned.1.call-done, f32[2048]{0:T(1024)S(1)} %bitcast.8, bf16[2048,4096]{1,0:T(8,128)(2,1)} %all-gather.3.cloned.1.call-done, f32[4096]{0:T(1024)S(1)} %copy-done.1, bf16[768,2048]{1,0:T(8,128)(2,1)S(1)} %copy-done, f32[2048]{0:T(1024)S(1)} %copy-done.3, ...), kind=kOutput, calls=%fused_computation.6 | convolution fusion | flops 25791823872 | bytes 39881728 | tf_op jit(solution)/shard_map/dot_general | solution.py:18
  490.8 0.0 reduce-scatter.2.cloned.1.call-update
  490.8 10.5 %reduce-scatter.2.cloned.1.call-done = bf16[768,1024]{1,0:T(8,128)(2,1)} async-done(((bf16[768,2048]{1,0:T(8,128)(2,1)}), bf16[768,1024]{1,0:T(8,128)(2,1)}) %reduce-scatter.2.cloned.1.call-update) | async-done | bytes 1572880 | tf_op jit(solution)/shard_map/reduce_scatter | solution.py:21
  (1 shorter events, 0.0 us)
Async XLA Ops:
  6.5 5.7 %copy-start = (bf16[768,2048]{1,0:T(8,128)(2,1)S(1)}, bf16[768,2048]{1,0:T(8,128)(2,1)}, u32[]{:S(2)}) copy-start(bf16[768,2048]{1,0:T(8,128)(2,1)} %param.6) | copy-start | bytes 9437188
  6.5 446.0 %copy-start.2 = (f32[1,2048]{1,0:T(1,128)S(1)}, f32[1,2048]{1,0:T(1,128)}, u32[]{:S(2)}) copy-start(f32[1,2048]{1,0:T(1,128)} %param.11) | copy-start | bytes 24580
  6.5 446.0 %copy-start.1 = (f32[4096]{0:T(1024)S(1)}, f32[4096]{0:T(1024)}, u32[]{:S(2)}) copy-start(f32[4096]{0:T(1024)} %param.9) | copy-start | bytes 49156
  6.5 446.0 %copy-start.3 = (f32[2048]{0:T(1024)S(1)}, f32[2048]{0:T(1024)}, u32[]{:S(2)}) copy-start(f32[2048]{0:T(1024)} %param.7) | copy-start | bytes 24580
  6.5 196.0 %all-gather.3.cloned.1.call-start = ((), (), s32[]{:S(2)}) async-start(), calls=%async_computation.1 | async-start | bytes 17825792 | tf_op jit(solution)/shard_map/all_gather | solution.py:14
  9.5 443.1 %all-gather.5.cloned.1.call-start = ((), (), s32[]{:S(2)}) async-start(), calls=%async_computation.2 | async-start | bytes 17825792 | tf_op jit(solution)/shard_map/all_gather | solution.py:17
  12.2 489.1 %reduce-scatter.2.cloned.1.call-start = ((), (), s32[]{:S(2)}) async-start(), calls=%async_computation.3 | async-start | bytes 4718592 | tf_op jit(solution)/shard_map/reduce_scatter | solution.py:21
Sparse Core Ops, SparseCore 0:
  10.1 192.3 all-gather.2
  205.2 247.2 all-gather.4
  491.0 10.3 reduce-scatter.1
where the time goes:
time: 508 us
  waiting for transfers between devices  450 us (89%)
  matrix products  38.3 us (8%)
  between operations  13.1 us (3%)
  other arithmetic  6.2 us (1%)
    all_gather x1, waiting for transfers between devices, on_device(): down_full = lax.all_gather(down_cast, 'fs', axis=1, tiled=True)  250 us
    all_gather x1, waiting for transfers between devices, on_device(): up_full = lax.all_gather(up_cast, 'fs', axis=0, tiled=True)  190 us
    dot_general x1, matrix products, on_device(): jnp.dot(hidden, down_full, preferred_element_type=jnp.float32) * down_scale  38.3 us
    reduce_scatter x1, waiting for transfers between devices, on_device(): lax.psum_scatter(rounded, 'tp', scatter_dimension=1, tiled=True)  10.5 us
  transfers between devices with their start and end apart: 3, of which 3 were waited for; matrix products, arithmetic and copies ran while one was open for 1% of the time, Pallas kernels for 0%

commit v1 on v0

--- a/solution.py
+++ b/solution.py
@@ -1,10 +1,20 @@
+import functools
+
 import jax
 import jax.numpy as jnp
 from jax import lax
+from jax.experimental import pallas as pl
+from jax.experimental.pallas import tpu as pltpu
 from jax.sharding import PartitionSpec as P
 
-
-def on_device(tokens, norm_gain, up_weight, up_scale, down_weight, down_scale):
+MESH = pl.DeviceIdType.MESH
+SIDE = 2
+GROUP = SIDE * SIDE
+CORES = 2
+COLS = 256
+
+
+def gathered(tokens, norm_gain, up_weight, up_scale, down_weight, down_scale):
     values = tokens.astype(jnp.float32)
     normed = (
         values * lax.rsqrt(jnp.mean(values * values, axis=-1, keepdims=True) + 1e-06) * norm_gain
@@ -24,9 +34,353 @@
     )
 
 
+def layer_kernel(
+    layers, rows, normed, up_in, down_in, up_scale, down_scale, out,
+    tok, upb, downb, hid, stage, partner, summed, peers, own,
+    local_sem, piece_recv, piece_send, level_send, tok_recv, tok_send,
+    mate_recv, mate_send, part_recv, part_send, red_recv, red_send,
+):
+    fs = lax.axis_index("fs")
+    core = lax.axis_index("tp")
+    z, q = fs // GROUP, fs % GROUP
+    depth, width = up_in.shape[0], upb.shape[1]
+    half = rows // CORES
+    sub = half // 2
+    units = 2 * layers
+    per_layer = GROUP * depth // COLS
+    per_unit = COLS // depth
+
+    def at(r):
+        return ((q // SIDE + r // SIDE) % SIDE) * SIDE + (q % SIDE + r % SIDE) % SIDE
+
+    def chip(layer, inner):
+        return (layer * GROUP + inner, core)
+
+    mate = (fs, 1 - core)
+
+    barrier = pltpu.get_barrier_semaphore()
+    for r in range(1, GROUP):
+        pl.semaphore_signal(barrier, inc=1, device_id=chip(z, at(r)), device_id_type=MESH)
+    pl.semaphore_signal(barrier, inc=1, device_id=mate, device_id_type=MESH)
+
+    @pl.when(z > 0)
+    def _():
+        pl.semaphore_signal(barrier, inc=1, device_id=chip(z - 1, q), device_id_type=MESH)
+
+    @pl.when(z < layers - 1)
+    def _():
+        pl.semaphore_signal(barrier, inc=1, device_id=chip(z + 1, q), device_id_type=MESH)
+
+    def slot(kind, layer, inner):
+        if kind == 0:
+            return upb.at[pl.ds(pl.multiple_of((layer * GROUP + inner) * depth, depth), depth), :]
+        return downb.at[layer, :, pl.ds(pl.multiple_of(inner * depth, depth), depth)]
+
+    def source(kind, inner):
+        if kind == 0:
+            return up_in.at[:, pl.ds(pl.multiple_of(inner * width, width), width)]
+        return down_in.at[pl.ds(pl.multiple_of(inner * width, width), width), :]
+
+    def remote(src, dst, send, recv, device):
+        return pltpu.make_async_remote_copy(
+            src_ref=src, dst_ref=dst, send_sem=send, recv_sem=recv,
+            device_id=device, device_id_type=MESH,
+        )
+
+    def along(kind, layer, inner, way):
+        piece = slot(kind, layer, inner)
+        index = layer * GROUP + inner
+        return remote(
+            piece, piece, piece_send.at[kind, index, way], piece_recv.at[kind, index],
+            chip(z + 2 * way - 1, q),
+        )
+
+    def level(kind, r):
+        return remote(
+            source(kind, at(r)), slot(kind, z, q), level_send.at[kind, r - 1],
+            piece_recv.at[kind, fs], chip(z, at(r)),
+        )
+
+    def each_way(kind, layer, inner, act):
+        @pl.when(jnp.logical_and(layer <= z, z < layers - 1))
+        def _():
+            act(along(kind, layer, inner, 1))
+
+        @pl.when(jnp.logical_and(layer >= z, z > 0))
+        def _():
+            act(along(kind, layer, inner, 0))
+
+    def start(copy):
+        copy.start()
+
+    def finish_send(copy):
+        copy.wait_send()
+
+    def arrived(kind, layer, inner):
+        piece = slot(kind, layer, inner)
+        remote(
+            piece, piece, piece_send.at[kind, layer * GROUP + inner, 0],
+            piece_recv.at[kind, layer * GROUP + inner], mate,
+        ).wait_recv()
+
+    def block(inner, side, s):
+        return tok.at[pl.ds(pl.multiple_of(inner * rows + side * half + s * sub, sub), sub), :]
+
+    def hand(r, s):
+        return remote(
+            normed.at[pl.ds(pl.multiple_of(core * half + s * sub, sub), sub), :],
+            block(q, core, s), tok_send.at[r - 1, s], tok_recv.at[r - 1, s], chip(z, at(r)),
+        )
+
+    def pass_on(came, to, s):
+        piece = block(at(came), core, s)
+        return remote(
+            piece, piece, tok_send.at[GROUP - 2, s], tok_recv.at[GROUP - 2, s], chip(z, at(to))
+        )
+
+    def tok_arrived(r, s):
+        piece = block(at(r), core, s)
+        remote(piece, piece, tok_send.at[r - 1, s], tok_recv.at[r - 1, s], mate).wait_recv()
+
+    def share(r, s):
+        piece = block(at(r), core, s)
+        return remote(piece, piece, mate_send.at[r - 1, s], mate_recv.at[r - 1, s], mate)
+
+    locals_ = [
+        pltpu.make_async_copy(source(0, q), slot(0, z, q), local_sem.at[0]),
+        pltpu.make_async_copy(source(1, q), slot(1, z, q), local_sem.at[1]),
+        pltpu.make_async_copy(
+            normed, tok.at[pl.ds(pl.multiple_of(q * rows, rows), rows), :], local_sem.at[2]
+        ),
+    ]
+    for copy in locals_:
+        copy.start()
+    greeted = GROUP + jnp.where(z > 0, 1, 0) + jnp.where(z < layers - 1, 1, 0)
+    pl.semaphore_wait(barrier, greeted)
+
+    for r in (3, 1, 2):
+        level(0, r).start()
+    hand(1, 0).start()
+    hand(2, 1).start()
+    hand(1, 1).start()
+    hand(2, 0).start()
+    for r in (3, 1, 2):
+        level(1, r).start()
+    for copy in locals_:
+        copy.wait()
+    each_way(0, z, q, start)
+    for r in (1, 2, 3):
+        arrived(0, z, at(r))
+        each_way(0, z, at(r), start)
+
+    def from_afar(d):
+        for r in range(GROUP):
+            @pl.when(z - d >= 0)
+            def _():
+                arrived(0, z - d, at(r))
+                each_way(0, z - d, at(r), start)
+
+            @pl.when(z + d < layers)
+            def _():
+                arrived(0, z + d, at(r))
+                each_way(0, z + d, at(r), start)
+
+    for d in range(1, layers):
+        from_afar(d)
+        if d == 1:
+            tok_arrived(1, 0)
+            pass_on(1, 2, 0).start()
+            share(1, 0).start()
+            tok_arrived(2, 1)
+            pass_on(2, 1, 1).start()
+            share(2, 1).start()
+
+    each_way(1, z, q, start)
+    for r in (1, 2, 3):
+        arrived(1, z, at(r))
+        each_way(1, z, at(r), start)
+    for r, s in ((1, 1), (2, 0), (3, 0), (3, 1)):
+        tok_arrived(r, s)
+        share(r, s).start()
+    for r in (1, 2, 3):
+        for s in (0, 1):
+            piece = block(at(r), 1 - core, s)
+            remote(piece, piece, mate_send.at[r - 1, s], mate_recv.at[r - 1, s], mate).wait_recv()
+
+    tall = rows * 2 // 3
+    wide = 256
+    across = width // wide
+
+    def first(i, carry):
+        m = pl.ds(pl.multiple_of((i // across) * tall, tall), tall)
+        at_n = pl.multiple_of((i % across) * wide, wide)
+        pre = jnp.dot(tok[m, :], upb[:, pl.ds(at_n, wide)], preferred_element_type=jnp.float32)
+        pre = pre * up_scale[:, pl.ds(pl.multiple_of(q * width + at_n, wide), wide)]
+        hid[m, pl.ds(at_n, wide)] = jnp.square(jnp.maximum(pre, 0.0)).astype(hid.dtype)
+        return carry
+
+    lax.fori_loop(0, (GROUP * rows // tall) * across, first, 0)
+
+    def red(u, r):
+        return remote(
+            summed.at[u, at(r)], peers.at[u, r - 1], red_send.at[u, r - 1],
+            red_recv.at[u, r - 1], chip(z, at(r)),
+        )
+
+    def part(u, b):
+        return remote(
+            stage.at[u, b], partner.at[u, b], part_send.at[u, b], part_recv.at[u, b], mate
+        )
+
+    def second(t, carry):
+        s, h = t // per_layer, t % per_layer
+        low = 2 * z < layers
+        layer = jnp.where(
+            low,
+            jnp.where(s <= z, z - s, s),
+            jnp.where(s <= layers - 1 - z, z + s, layers - 1 - s),
+        )
+
+        @pl.when(s > 0)
+        def _():
+            for k in range(per_unit):
+                arrived(1, layer, h * per_unit + k)
+                each_way(1, layer, h * per_unit + k, start)
+
+        unit = layer * per_layer + h
+        owner = unit // (units // CORES)
+        u = unit % (units // CORES)
+        cols = pl.ds(pl.multiple_of(h * COLS, COLS), COLS)
+        scale = pl.ds(pl.multiple_of(unit * COLS, COLS), COLS)
+
+        def product(b):
+            m = pl.ds(pl.multiple_of(b * rows, rows), rows)
+            value = jnp.dot(hid[m, :], downb[layer, :, cols], preferred_element_type=jnp.float32)
+            return value * down_scale[:, scale]
+
+        @pl.when(owner != core)
+        def _():
+            def away(i, c):
+                b = at(GROUP - 1 - i)
+                stage[u, b] = product(b).astype(stage.dtype)
+                part(u, b).start()
+                return c
+
+            lax.fori_loop(0, GROUP, away, 0)
+
+        @pl.when(owner == core)
+        def _():
+            def mine(i, c):
+                own[at(GROUP - 1 - i)] = product(at(GROUP - 1 - i))
+                return c
+
+            lax.fori_loop(0, GROUP, mine, 0)
+            for r in (3, 2, 1, 0):
+                b = at(r)
+                part(u, b).wait_recv()
+                summed[u, b] = (own[b] + partner[u, b].astype(jnp.float32)).astype(summed.dtype)
+                if r:
+                    red(u, r).start()
+
+        return carry
+
+    lax.fori_loop(0, units, second, 0)
+
+    def last(u, carry):
+        for r in range(1, GROUP):
+            red(u, r).wait_recv()
+        total = summed[u, q].astype(jnp.float32)
+        for r in range(1, GROUP):
+            total = total + peers[u, r - 1].astype(jnp.float32)
+        out[:, pl.ds(pl.multiple_of(u * COLS, COLS), COLS)] = total.astype(out.dtype)
+        return carry
+
+    lax.fori_loop(0, units // CORES, last, 0)
+
+    def drain(u, carry):
+        for r in range(1, GROUP):
+            red(u, r).wait_send()
+        for b in range(GROUP):
+            part(u, b).wait_send()
+        return carry
+
+    lax.fori_loop(0, units // CORES, drain, 0)
+    for kind in (0, 1):
+        for r in range(1, GROUP):
+            level(kind, r).wait_send()
+
+        def drained(i, carry):
+            each_way(kind, i // GROUP, i % GROUP, finish_send)
+            return carry
+
+        lax.fori_loop(0, layers * GROUP, drained, 0)
+    for r in (1, 2):
+        for s in (0, 1):
+            hand(r, s).wait_send()
+    pass_on(1, 2, 0).wait_send()
+    pass_on(2, 1, 1).wait_send()
+    for r in (1, 2, 3):
+        for s in (0, 1):
+            share(r, s).wait_send()
+
+
+def grouped(layers, tokens, norm_gain, up_weight, up_scale, down_weight, down_scale):
+    values = tokens.astype(jnp.float32)
+    normed = (
+        values * lax.rsqrt(jnp.mean(values * values, axis=-1, keepdims=True) + 1e-06) * norm_gain
+    ).astype(jnp.bfloat16)
+    up_cast = up_weight.astype(jnp.bfloat16)
+    down_cast = down_weight.astype(jnp.bfloat16)
+    rows, model = tokens.shape
+    depth = up_weight.shape[0]
+    width = up_weight.shape[1] // GROUP
+    share = model // COLS // CORES
+    n = layers * GROUP
+    dma = pltpu.SemaphoreType.DMA
+    vmem = pl.BlockSpec(memory_space=pltpu.VMEM)
+    hbm = pl.BlockSpec(memory_space=pltpu.HBM)
+    return pl.pallas_call(
+        functools.partial(layer_kernel, layers, rows),
+        out_shape=jax.ShapeDtypeStruct((rows, model // CORES), jnp.bfloat16),
+        in_specs=[hbm, hbm, hbm, vmem, vmem],
+        out_specs=vmem,
+        scratch_shapes=[
+            pltpu.VMEM((GROUP * rows, model), jnp.bfloat16),
+            pltpu.VMEM((model, width), jnp.bfloat16),
+            pltpu.VMEM((layers, width, GROUP * depth), jnp.bfloat16),
+            pltpu.VMEM((GROUP * rows, width), jnp.bfloat16),
+            pltpu.VMEM((share, GROUP, rows, COLS), jnp.bfloat16),
+            pltpu.VMEM((share, GROUP, rows, COLS), jnp.bfloat16),
+            pltpu.VMEM((share, GROUP, rows, COLS), jnp.bfloat16),
+            pltpu.VMEM((share, GROUP - 1, rows, COLS), jnp.bfloat16),
+            pltpu.VMEM((GROUP, rows, COLS), jnp.float32),
+            dma((3,)),
+            dma((2, n)),
+            dma((2, n, 2)),
+            dma((2, GROUP - 1)),
+            dma((GROUP - 1, 2)),
+            dma((GROUP - 1, 2)),
+            dma((GROUP - 1, 2)),
+            dma((GROUP - 1, 2)),
+            dma((share, GROUP)),
+            dma((share, GROUP)),
+            dma((share, GROUP - 1)),
+            dma((share, GROUP - 1)),
+        ],
+        compiler_params=pltpu.CompilerParams(
+            collective_id=0, has_side_effects=True, vmem_limit_bytes=62 * 2**20
+        ),
+    )(normed, up_cast, down_cast, up_scale.reshape(1, -1), down_scale)
+
+
 def solution(mesh):
+    fs, tp = mesh.shape["fs"], mesh.shape["tp"]
+    if tp == CORES and fs % (2 * GROUP) == 0 and fs <= 4 * GROUP:
+        body = functools.partial(grouped, fs // GROUP)
+    else:
+        body = gathered
     in_specs = (P("fs", None), P(), P("fs", "tp"), P("tp"), P("tp", "fs"), P())
     out_specs = P("fs", "tp")
     return jax.shard_map(
-        on_device, mesh=mesh, in_specs=in_specs, out_specs=out_specs, check_vma=False
+        body, mesh=mesh, in_specs=in_specs, out_specs=out_specs, check_vma=False
     )

time: 508 us -> 193 us (0.38)
  waiting for transfers between devices: 450 us -> 0 us
  Pallas kernels: 0 us -> 182 us
  matrix products: 38.3 us -> 0 us
  between operations: 13.1 us -> 0.04 us
    all_gather x2 -> x0, waiting for transfers between devices: 440 us -> none  [the longest x1 250 us: on_device(): down_full = lax.all_gather(down_cast, 'fs', axis=1, tiled=True)]
    pallas_call x0 -> x1, Pallas kernels: none -> 182 us  [grouped(): pl.pallas_call(functools.partial(layer_kernel, layers, rows), out_shape=j...]
    dot_general x1 -> x0, matrix products: 38.3 us -> none  [on_device(): jnp.dot(hidden, down_full, preferred_element_type=jnp.float32) * down_scale]
    reduce_scatter x1 -> x0, waiting for transfers between devices: 10.5 us -> none  [on_device(): lax.psum_scatter(rounded, 'tp', scatter_dimension=1, tiled=True)]
  transfers between devices with their start and end apart: 3 -> 0, of which waited for: 3 -> 0; matrix products, arithmetic and copies ran while one was open for 1% -> 0% of each run, Pallas kernels for 0% -> 0%
where the time goes in v1:
time: 193 us
  Pallas kernels  182 us (94%)
  other arithmetic  7.4 us (4%)
  local copies, waits for them, and re-layouts  2.98 us (2%)
    pallas_call x1, Pallas kernels, grouped(): pl.pallas_call(functools.partial(layer_kernel, layers, rows), out_shape=j...  182 us

profile of v1, /device:TPU:1, one launch (start us, length us, event | category | flops | bytes accessed | tf_op | source)
XLA Modules:
  0.0 192.5 jit_solution(10326717620847425174)
XLA Ops:
  0.0 0.0 copy-start.1
  0.0 0.0 copy-start.2
  0.0 2.7 %fusion = f32[768]{0:T(1024)S(1)} fusion(bf16[768,2048]{1,0:T(8,128)(2,1)} %param.6), kind=kLoop, calls=%fused_computation.2 | loop fusion | flops 4717824 | bytes 3148800 | tf_op jit(solution)/shard_map/reduce_sum | solution.py:330
  2.7 0.0 copy-done.1
  2.7 0.0 copy-start
  2.8 0.0 copy-start.3
  2.8 1.1 convert_element_type.14.up_in
  3.9 0.0 copy-done.2
  3.9 1.1 convert_element_type.15.down_in
  5.0 0.3 copy-done
  5.3 0.0 copy-done.3
  5.3 2.4 %fusion.2.normed = bf16[768,2048]{1,0:T(8,128)(2,1)} fusion(bf16[768,2048]{1,0:T(8,128)(2,1)S(1)} %copy-done, f32[2048]{0:T(1024)S(1)} %copy-done.3, f32[768]{0:T(1024)S(1)} %add_rsqrt_fusion), kind=kLoop, calls=%fused_computation.4 | loop fusion | flops 6291456 | bytes 6302720 | tf_op jit(solution)/shard_map/convert_element_type | solution.py:331
  7.7 182.1 %shard_map.64 = bf16[768,1024]{1,0:T(8,128)(2,1)} custom-call(bf16[768,2048]{1,0:T(8,128)(2,1)} %fusion.2.normed, bf16[128,4096]{1,0:T(8,128)(2,1)} %convert_element_type.14.up_in, bf16[4096,128]{1,0:T(8,128)(2,1)} %convert_element_type.15.down_in, f32[1,4096]{1,0:T(1,128)} %bitcast.1, f32[1,2048]{1,0:T(1,128)} %down_scale.1), custom_call_target="tpu_custom_call" | custom-call | tf_op jit(solution)/shard_map/pallas_call | solution.py:342
  189.8 2.7 %copy.8 = bf16[768,1024]{1,0:T(8,128)(2,1)} copy(bf16[768,1024]{1,0:T(8,128)(2,1)} %shard_map.64) | data formatting | bytes 3145728
  (1 shorter events, 0.0 us)
Async XLA Ops:
  0.0 2.7 %copy-start.1 = (f32[128,4096]{1,0:T(8,128)S(1)}, f32[128,4096]{1,0:T(8,128)}, u32[]{:S(2)}) copy-start(f32[128,4096]{1,0:T(8,128)} %param.8) | copy-start | bytes 6291460
  0.0 3.9 %copy-start.2 = (f32[4096,128]{1,0:T(8,128)S(1)}, f32[4096,128]{1,0:T(8,128)}, u32[]{:S(2)}) copy-start(f32[4096,128]{1,0:T(8,128)} %param.10) | copy-start | bytes 6291460
  2.7 2.5 %copy-start = (bf16[768,2048]{1,0:T(8,128)(2,1)S(1)}, bf16[768,2048]{1,0:T(8,128)(2,1)}, u32[]{:S(2)}) copy-start(bf16[768,2048]{1,0:T(8,128)(2,1)} %param.6) | copy-start | bytes 9437188
  2.8 2.5 %copy-start.3 = (f32[2048]{0:T(1024)S(1)}, f32[2048]{0:T(1024)}, u32[]{:S(2)}) copy-start(f32[2048]{0:T(1024)} %param.7) | copy-start | bytes 24580

commit v2 on v1

--- a/solution.py
+++ b/solution.py
@@ -12,6 +12,7 @@
 GROUP = SIDE * SIDE
 CORES = 2
 COLS = 256
+STRIP = 32
 
 
 def gathered(tokens, norm_gain, up_weight, up_scale, down_weight, down_scale):
@@ -35,7 +36,7 @@
 
 
 def layer_kernel(
-    layers, rows, normed, up_in, down_in, up_scale, down_scale, out,
+    layers, rows, tokens, gain, up_in, down_in, up_scale, down_scale, out,
     tok, upb, downb, hid, stage, partner, summed, peers, own,
     local_sem, piece_recv, piece_send, level_send, tok_recv, tok_send,
     mate_recv, mate_send, part_recv, part_send, red_recv, red_send,
@@ -127,10 +128,8 @@
         return tok.at[pl.ds(pl.multiple_of(inner * rows + side * half + s * sub, sub), sub), :]
 
     def hand(r, s):
-        return remote(
-            normed.at[pl.ds(pl.multiple_of(core * half + s * sub, sub), sub), :],
-            block(q, core, s), tok_send.at[r - 1, s], tok_recv.at[r - 1, s], chip(z, at(r)),
-        )
+        piece = block(q, core, s)
+        return remote(piece, piece, tok_send.at[r - 1, s], tok_recv.at[r - 1, s], chip(z, at(r)))
 
     def pass_on(came, to, s):
         piece = block(at(came), core, s)
@@ -144,14 +143,14 @@
 
     def share(r, s):
         piece = block(at(r), core, s)
-        return remote(piece, piece, mate_send.at[r - 1, s], mate_recv.at[r - 1, s], mate)
-
+        return remote(piece, piece, mate_send.at[r, s], mate_recv.at[r, s], mate)
+
+    half_at = pl.ds(pl.multiple_of(q * rows + core * half, half), half)
+    mine_at = pl.ds(pl.multiple_of(core * half, half), half)
     locals_ = [
         pltpu.make_async_copy(source(0, q), slot(0, z, q), local_sem.at[0]),
         pltpu.make_async_copy(source(1, q), slot(1, z, q), local_sem.at[1]),
-        pltpu.make_async_copy(
-            normed, tok.at[pl.ds(pl.multiple_of(q * rows, rows), rows), :], local_sem.at[2]
-        ),
+        pltpu.make_async_copy(tokens.at[mine_at, :], tok.at[half_at, :], local_sem.at[2]),
     ]
     for copy in locals_:
         copy.start()
@@ -160,15 +159,24 @@
 
     for r in (3, 1, 2):
         level(0, r).start()
+    for copy in locals_:
+        copy.wait()
+    each_way(0, z, q, start)
+
+    def normalize(i, carry):
+        strip = pl.ds(pl.multiple_of(q * rows + core * half + i * STRIP, STRIP), STRIP)
+        values = tok[strip, :].astype(jnp.float32)
+        mean = jnp.mean(values * values, axis=-1, keepdims=True)
+        tok[strip, :] = (values * lax.rsqrt(mean + 1e-06) * gain[...]).astype(tok.dtype)
+        return carry
+
+    lax.fori_loop(0, half // STRIP, normalize, 0)
     hand(1, 0).start()
     hand(2, 1).start()
     hand(1, 1).start()
     hand(2, 0).start()
-    for r in (3, 1, 2):
-        level(1, r).start()
-    for copy in locals_:
-        copy.wait()
-    each_way(0, z, q, start)
+    for s in (0, 1):
+        share(0, s).start()
     for r in (1, 2, 3):
         arrived(0, z, at(r))
         each_way(0, z, at(r), start)
@@ -194,6 +202,8 @@
             tok_arrived(2, 1)
             pass_on(2, 1, 1).start()
             share(2, 1).start()
+            for r in (3, 1, 2):
+                level(1, r).start()
 
     each_way(1, z, q, start)
     for r in (1, 2, 3):
@@ -202,10 +212,10 @@
     for r, s in ((1, 1), (2, 0), (3, 0), (3, 1)):
         tok_arrived(r, s)
         share(r, s).start()
-    for r in (1, 2, 3):
+    for r in (0, 1, 2, 3):
         for s in (0, 1):
             piece = block(at(r), 1 - core, s)
-            remote(piece, piece, mate_send.at[r - 1, s], mate_recv.at[r - 1, s], mate).wait_recv()
+            remote(piece, piece, mate_send.at[r, s], mate_recv.at[r, s], mate).wait_recv()
 
     tall = rows * 2 // 3
     wide = 256
@@ -221,11 +231,34 @@
 
     lax.fori_loop(0, (GROUP * rows // tall) * across, first, 0)
 
-    def red(u, r):
+    upper, lower = pl.ds(0, half), pl.ds(half, half)
+    hops = ((3, upper, 2, 1), (3, lower, 2, 2), (1, upper, 0, 1), (2, lower, 1, 2),
+            (1, lower, 0, 1), (2, upper, 1, 2))
+
+    def red(u, k):
+        of, part_rows, into, to = hops[k]
         return remote(
-            summed.at[u, at(r)], peers.at[u, r - 1], red_send.at[u, r - 1],
-            red_recv.at[u, r - 1], chip(z, at(r)),
-        )
+            summed.at[u, at(of), part_rows, :], peers.at[u, into, part_rows, :],
+            red_send.at[u, k], red_recv.at[u, k], chip(z, at(to)),
+        )
+
+    def relay(u):
+        for k, of, part_rows, then in ((0, 2, upper, 5), (1, 1, lower, 4)):
+            red(u, k).wait_recv()
+            total = summed[u, at(of), part_rows, :].astype(jnp.float32)
+            total = total + peers[u, 2, part_rows, :].astype(jnp.float32)
+            summed[u, at(of), part_rows, :] = total.astype(summed.dtype)
+            red(u, then).start()
+
+    def unit_of(t):
+        s, h = t // per_layer, t % per_layer
+        layer = jnp.where(
+            2 * z < layers,
+            jnp.where(s <= z, z - s, s),
+            jnp.where(s <= layers - 1 - z, z + s, layers - 1 - s),
+        )
+        unit = layer * per_layer + h
+        return s, h, layer, unit, unit // (units // CORES), unit % (units // CORES)
 
     def part(u, b):
         return remote(
@@ -233,13 +266,7 @@
         )
 
     def second(t, carry):
-        s, h = t // per_layer, t % per_layer
-        low = 2 * z < layers
-        layer = jnp.where(
-            low,
-            jnp.where(s <= z, z - s, s),
-            jnp.where(s <= layers - 1 - z, z + s, layers - 1 - s),
-        )
+        s, h, layer, unit, owner, u = unit_of(t)
 
         @pl.when(s > 0)
         def _():
@@ -247,9 +274,6 @@
                 arrived(1, layer, h * per_unit + k)
                 each_way(1, layer, h * per_unit + k, start)
 
-        unit = layer * per_layer + h
-        owner = unit // (units // CORES)
-        u = unit % (units // CORES)
         cols = pl.ds(pl.multiple_of(h * COLS, COLS), COLS)
         scale = pl.ds(pl.multiple_of(unit * COLS, COLS), COLS)
 
@@ -279,27 +303,38 @@
                 b = at(r)
                 part(u, b).wait_recv()
                 summed[u, b] = (own[b] + partner[u, b].astype(jnp.float32)).astype(summed.dtype)
-                if r:
-                    red(u, r).start()
+                for k in {3: (0, 1), 1: (2,), 2: (3,), 0: ()}[r]:
+                    red(u, k).start()
+
+        before = unit_of(jnp.maximum(t - 1, 0))
+
+        @pl.when(jnp.logical_and(t > 0, before[4] == core))
+        def _():
+            relay(before[5])
 
         return carry
 
     lax.fori_loop(0, units, second, 0)
+    final = unit_of(units - 1)
+
+    @pl.when(final[4] == core)
+    def _():
+        relay(final[5])
 
     def last(u, carry):
-        for r in range(1, GROUP):
-            red(u, r).wait_recv()
+        for k in range(2, 6):
+            red(u, k).wait_recv()
         total = summed[u, q].astype(jnp.float32)
-        for r in range(1, GROUP):
-            total = total + peers[u, r - 1].astype(jnp.float32)
+        for side in range(2):
+            total = total + peers[u, side].astype(jnp.float32)
         out[:, pl.ds(pl.multiple_of(u * COLS, COLS), COLS)] = total.astype(out.dtype)
         return carry
 
     lax.fori_loop(0, units // CORES, last, 0)
 
     def drain(u, carry):
-        for r in range(1, GROUP):
-            red(u, r).wait_send()
+        for k in range(len(hops)):
+            red(u, k).wait_send()
         for b in range(GROUP):
             part(u, b).wait_send()
         return carry
@@ -319,16 +354,12 @@
             hand(r, s).wait_send()
     pass_on(1, 2, 0).wait_send()
     pass_on(2, 1, 1).wait_send()
-    for r in (1, 2, 3):
+    for r in (0, 1, 2, 3):
         for s in (0, 1):
             share(r, s).wait_send()
 
 
 def grouped(layers, tokens, norm_gain, up_weight, up_scale, down_weight, down_scale):
-    values = tokens.astype(jnp.float32)
-    normed = (
-        values * lax.rsqrt(jnp.mean(values * values, axis=-1, keepdims=True) + 1e-06) * norm_gain
-    ).astype(jnp.bfloat16)
     up_cast = up_weight.astype(jnp.bfloat16)
     down_cast = down_weight.astype(jnp.bfloat16)
     rows, model = tokens.shape
@@ -342,7 +373,7 @@
     return pl.pallas_call(
         functools.partial(layer_kernel, layers, rows),
         out_shape=jax.ShapeDtypeStruct((rows, model // CORES), jnp.bfloat16),
-        in_specs=[hbm, hbm, hbm, vmem, vmem],
+        in_specs=[hbm, vmem, hbm, hbm, vmem, vmem],
         out_specs=vmem,
         scratch_shapes=[
             pltpu.VMEM((GROUP * rows, model), jnp.bfloat16),
@@ -360,17 +391,17 @@
             dma((2, GROUP - 1)),
             dma((GROUP - 1, 2)),
             dma((GROUP - 1, 2)),
-            dma((GROUP - 1, 2)),
-            dma((GROUP - 1, 2)),
+            dma((GROUP, 2)),
+            dma((GROUP, 2)),
             dma((share, GROUP)),
             dma((share, GROUP)),
-            dma((share, GROUP - 1)),
-            dma((share, GROUP - 1)),
+            dma((share, 6)),
+            dma((share, 6)),
         ],
         compiler_params=pltpu.CompilerParams(
             collective_id=0, has_side_effects=True, vmem_limit_bytes=62 * 2**20
         ),
-    )(normed, up_cast, down_cast, up_scale.reshape(1, -1), down_scale)
+    )(tokens, norm_gain.reshape(1, -1), up_cast, down_cast, up_scale.reshape(1, -1), down_scale)
 
 
 def solution(mesh):

time: 193 us -> 185 us (0.959)
  Pallas kernels: 182 us -> 178 us
  other arithmetic: 7.4 us -> 3.92 us
    pallas_call x1, Pallas kernels: 182 us -> 178 us  [grouped(): pl.pallas_call(functools.partial(layer_kernel, layers, rows), out_shape=j...]
    reduce_sum x1 -> x0, other arithmetic: 2.72 us -> none  [grouped(): jnp.mean(values * values, axis=-1, keepdims=True) + 1e-06]
    convert_element_type x1 -> x0, other arithmetic: 2.44 us -> none  [grouped(): normed = (values * lax.rsqrt(jnp.mean(values * values, axis=-1, keepdims=...]
where the time goes in v2:
time: 185 us
  Pallas kernels  178 us (96%)
  other arithmetic  3.92 us (2%)
  local copies, waits for them, and re-layouts  2.67 us (1%)
    pallas_call x1, Pallas kernels, grouped(): pl.pallas_call(functools.partial(layer_kernel, layers, rows), out_shape=j...  178 us

profile of v2, /device:TPU:1, one launch (start us, length us, event | category | flops | bytes accessed | tf_op | source)
XLA Modules:
  0.0 184.6 jit_solution(80461728208594229)
XLA Ops:
  0.0 0.0 copy-start
  0.0 2.8 %convert_element_type.6.up_in = bf16[128,4096]{1,0:T(8,128)(2,1)} convert(f32[128,4096]{1,0:T(8,128)} %param.8) | non-fusion elementwise | flops 524288 | bytes 3145728 | tf_op jit(solution)/shard_map/convert_element_type | solution.py:363
  2.8 0.0 copy-done
  2.8 1.1 convert_element_type.7.down_in
  3.9 178.0 %shard_map.64 = bf16[768,1024]{1,0:T(8,128)(2,1)} custom-call(bf16[768,2048]{1,0:T(8,128)(2,1)} %tokens.1, f32[1,2048]{1,0:T(1,128)} %bitcast.3, bf16[128,4096]{1,0:T(8,128)(2,1)} %convert_element_type.6.up_in, bf16[4096,128]{1,0:T(8,128)(2,1)} %convert_element_type.7.down_in, f32[1,4096]{1,0:T(1,128)} %bitcast.2, f32[1,2048]{1,0:T(1,128)} %down_scale.1), custom_call_target="tpu_custom_call" | custom-call | tf_op jit(solution)/shard_map/pallas_call | solution.py:373
  181.9 2.7 %copy.8 = bf16[768,1024]{1,0:T(8,128)(2,1)} copy(bf16[768,1024]{1,0:T(8,128)(2,1)} %shard_map.64) | data formatting | bytes 3145728
Async XLA Ops:
  0.0 2.8 %copy-start = (f32[4096,128]{1,0:T(8,128)S(1)}, f32[4096,128]{1,0:T(8,128)}, u32[]{:S(2)}) copy-start(f32[4096,128]{1,0:T(8,128)} %param.10) | copy-start | bytes 6291460

commit v3 on v2

--- a/solution.py
+++ b/solution.py
@@ -175,6 +175,8 @@
     hand(2, 1).start()
     hand(1, 1).start()
     hand(2, 0).start()
+    for r in (3, 1, 2):
+        level(1, r).start()
     for s in (0, 1):
         share(0, s).start()
     for r in (1, 2, 3):
@@ -202,13 +204,16 @@
             tok_arrived(2, 1)
             pass_on(2, 1, 1).start()
             share(2, 1).start()
-            for r in (3, 1, 2):
-                level(1, r).start()
-
-    each_way(1, z, q, start)
-    for r in (1, 2, 3):
-        arrived(1, z, at(r))
-        each_way(1, z, at(r), start)
+            for r in (1, 2, 3):
+                arrived(1, z, at(r))
+        for way, ahead in ((1, z), (0, layers - 1 - z)):
+            due = ahead <= 1 if d == 1 else ahead == d
+
+            @pl.when(jnp.logical_and(due, (layers - 1 - z if way else z) > 0))
+            def _():
+                for r in range(GROUP):
+                    along(1, z, at(r), way).start()
+
     for r, s in ((1, 1), (2, 0), (3, 0), (3, 1)):
         tok_arrived(r, s)
         share(r, s).start()
@@ -229,7 +234,23 @@
         hid[m, pl.ds(at_n, wide)] = jnp.square(jnp.maximum(pre, 0.0)).astype(hid.dtype)
         return carry
 
-    lax.fori_loop(0, (GROUP * rows // tall) * across, first, 0)
+    def take(d, r):
+        for layer, there in ((z - d, z - d >= 0), (z + d, z + d < layers)):
+            @pl.when(there)
+            def _():
+                arrived(1, layer, r)
+                each_way(1, layer, r, start)
+
+    inside = jnp.logical_and(z > 0, z < layers - 1)
+    tiles = (GROUP * rows // tall) * across
+    lax.fori_loop(0, tiles // 2, first, 0)
+
+    @pl.when(inside)
+    def _():
+        for r in range(GROUP):
+            take(1, r)
+
+    lax.fori_loop(tiles // 2, tiles, first, 0)
 
     upper, lower = pl.ds(0, half), pl.ds(half, half)
     hops = ((3, upper, 2, 1), (3, lower, 2, 2), (1, upper, 0, 1), (2, lower, 1, 2),
@@ -268,11 +289,12 @@
     def second(t, carry):
         s, h, layer, unit, owner, u = unit_of(t)
 
-        @pl.when(s > 0)
+        d = s + jnp.where(inside, 1, 0)
+
+        @pl.when(d > jnp.where(inside, 1, 0))
         def _():
             for k in range(per_unit):
-                arrived(1, layer, h * per_unit + k)
-                each_way(1, layer, h * per_unit + k, start)
+                take(d, h * per_unit + k)
 
         cols = pl.ds(pl.multiple_of(h * COLS, COLS), COLS)
         scale = pl.ds(pl.multiple_of(unit * COLS, COLS), COLS)

time: 185 us -> 178 us (0.962)
  Pallas kernels: 178 us -> 171 us
    pallas_call x1, Pallas kernels: 178 us -> 171 us  [grouped(): pl.pallas_call(functools.partial(layer_kernel, layers, rows), out_shape=j...]
where the time goes in v3:
time: 178 us
  Pallas kernels  171 us (96%)
  other arithmetic  3.92 us (2%)
  local copies, waits for them, and re-layouts  2.67 us (2%)
    pallas_call x1, Pallas kernels, grouped(): pl.pallas_call(functools.partial(layer_kernel, layers, rows), out_shape=j...  171 us

profile of v3, /device:TPU:1, one launch (start us, length us, event | category | flops | bytes accessed | tf_op | source)
XLA Modules:
  0.0 177.6 jit_solution(8349243237796239351)
XLA Ops:
  0.0 0.0 copy-start
  0.0 2.8 %convert_element_type.6.up_in = bf16[128,4096]{1,0:T(8,128)(2,1)} convert(f32[128,4096]{1,0:T(8,128)} %param.8) | non-fusion elementwise | flops 524288 | bytes 3145728 | tf_op jit(solution)/shard_map/convert_element_type | solution.py:385
  2.8 0.0 copy-done
  2.8 1.1 convert_element_type.7.down_in
  3.9 171.0 %shard_map.64 = bf16[768,1024]{1,0:T(8,128)(2,1)} custom-call(bf16[768,2048]{1,0:T(8,128)(2,1)} %tokens.1, f32[1,2048]{1,0:T(1,128)} %bitcast.3, bf16[128,4096]{1,0:T(8,128)(2,1)} %convert_element_type.6.up_in, bf16[4096,128]{1,0:T(8,128)(2,1)} %convert_element_type.7.down_in, f32[1,4096]{1,0:T(1,128)} %bitcast.2, f32[1,2048]{1,0:T(1,128)} %down_scale.1), custom_call_target="tpu_custom_call" | custom-call | tf_op jit(solution)/shard_map/pallas_call | solution.py:395
  174.9 2.7 %copy.8 = bf16[768,1024]{1,0:T(8,128)(2,1)} copy(bf16[768,1024]{1,0:T(8,128)(2,1)} %shard_map.64) | data formatting | bytes 3145728
Async XLA Ops:
  0.0 2.8 %copy-start = (f32[4096,128]{1,0:T(8,128)S(1)}, f32[4096,128]{1,0:T(8,128)}, u32[]{:S(2)}) copy-start(f32[4096,128]{1,0:T(8,128)} %param.10) | copy-start | bytes 6291460
